TPU v7x, 32 devices: a whole 2x2x4 slice. The times are simulated.
32 devices in a mesh: grp: 2 (over y), sp: 4 (over z), tp: 4 (over x, core).
Axes of the slice: x: 2, y: 2, z: 4, core: 2. Of those that a mesh axis runs over, the one named last changes fastest.
Arguments:
- queries: bfloat16 [6144, 1024], P(('grp', 'sp'), 'tp'), parts along dimension 0, may hold values from -160 to 160
- key_rows: bfloat16 [6144, 256], P(('grp', 'sp'), 'tp'), parts along dimension 0, may hold values from -4 to 4
- value_rows: bfloat16 [6144, 256], P(('grp', 'sp'), 'tp'), parts along dimension 0, may hold values from -5 to 5
- sink_logits: float32 [16], P('tp'), may hold values from 2 to 6
- out_weight: bfloat16 [1024, 2048], replicated, may hold values from -0.75 to 0.75
- residual: bfloat16 [6144, 2048], P(('grp', 'sp', 'tp')), parts along dimension 0, may hold values from -6 to 6
- norm_gain: float32 [2048], replicated, may hold values from 0.1 to 1.9
- up_weight: bfloat16 [2048, 4096], P('sp', 'tp'), may hold values from -0.125 to 0.125
- down_weight: bfloat16 [4096, 2048], P('tp', 'sp'), may hold values from -0.09375 to 0.09375
Outputs:
- layer_out: bfloat16 [6144, 2048], P(('grp', 'sp', 'tp')), parts along dimension 0
There are 2 independent parts, one for each index of `grp`. A program takes and returns all parts, laid end to end along the dimension named above; an argument that names none is the same for every part. Nothing has to cross between parts.
All inputs are finite; a program needn't handle non-finite values.
Results may differ from a plain program's by a relative error of at most 0.017.
Values may be sent and summed in bfloat16 or wider, within the bound.
A program may use at most 64 MiB of HBM per device.

v0:
```python
import functools

import jax
import jax.numpy as jnp
from jax import lax
from jax.experimental import pallas as pl
from jax.experimental.pallas import tpu as pltpu
from jax.sharding import PartitionSpec as P

HEAD_DIM = 64
WINDOW = 128


def shifted(value, axis, steps):
    count = lax.axis_size(axis)
    leading, last = (max(0, -steps), min(count, count - steps))
    return lax.ppermute(value, axis, [(source, source + steps) for source in range(leading, last)])


def band_attend(queries, key_rows, value_rows, sink_logits, tail_keys, tail_values, offset):
    rows = queries.shape[0]
    kv_heads = key_rows.shape[1] // HEAD_DIM
    group = queries.shape[1] // (kv_heads * HEAD_DIM)
    blocks = rows // WINDOW
    all_keys = jnp.concatenate([tail_keys, key_rows], axis=0).reshape(
        blocks + 1, WINDOW, kv_heads, HEAD_DIM
    )
    all_values = jnp.concatenate([tail_values, value_rows], axis=0).reshape(
        blocks + 1, WINDOW, kv_heads, HEAD_DIM
    )
    key_blocks = jnp.concatenate([all_keys[:-1], all_keys[1:]], axis=1)
    value_blocks = jnp.concatenate([all_values[:-1], all_values[1:]], axis=1)
    query_blocks = queries.reshape(blocks, WINDOW, kv_heads, group, HEAD_DIM)
    scores = jnp.einsum(
        "nqkgd,nskd->nkgqs", query_blocks, key_blocks, preferred_element_type=jnp.float32
    ) * HEAD_DIM ** (-0.5)
    q_local = jnp.arange(WINDOW, dtype=jnp.int32) + WINDOW
    k_local = jnp.arange(2 * WINDOW, dtype=jnp.int32)
    distance = q_local[:, None] - k_local[None, :]
    key_position = (
        offset + (jnp.arange(blocks, dtype=jnp.int32)[:, None] - 1) * WINDOW + k_local[None, :]
    )
    valid = ((distance >= 0) & (distance < WINDOW))[None] & (key_position >= 0)[:, None, :]
    scores = jnp.where(valid[:, None, None], scores, -1e30)
    sink = sink_logits.reshape(kv_heads, group)[None, :, :, None, None]
    top = jnp.maximum(jnp.max(scores, axis=-1, keepdims=True), sink)
    weights = jnp.exp(scores - top)
    total = jnp.sum(weights, axis=-1, keepdims=True) + jnp.exp(sink - top)
    probs = (weights / total).astype(jnp.bfloat16)
    result = jnp.einsum(
        "nkgqs,nskd->nqkgd", probs, value_blocks, preferred_element_type=jnp.float32
    )
    return result.astype(jnp.bfloat16).reshape(rows, kv_heads * group * HEAD_DIM)


def body(
    queries,
    key_rows,
    value_rows,
    sink_logits,
    out_weight,
    residual,
    norm_gain,
    up_weight,
    down_weight,
):
    rows = queries.shape[0]
    width = key_rows.shape[1]
    kv_pair = jnp.concatenate([key_rows[rows - WINDOW :], value_rows[rows - WINDOW :]], axis=1)
    tail = shifted(kv_pair, "sp", 1)
    offset = lax.axis_index("sp") * rows
    attended = band_attend(
        queries, key_rows, value_rows, sink_logits, tail[:, :width], tail[:, width:], offset
    )
    head_cols = attended.shape[1]
    own_rows = lax.dynamic_slice_in_dim(out_weight, lax.axis_index("tp") * head_cols, head_cols, 0)
    projected = lax.psum_scatter(
        jnp.dot(attended, own_rows, preferred_element_type=jnp.float32).astype(jnp.bfloat16),
        "tp",
        scatter_dimension=0,
        tiled=True,
    ).astype(jnp.float32)
    mixed32 = (residual.astype(jnp.float32) + projected).astype(jnp.bfloat16).astype(jnp.float32)
    scale = lax.rsqrt(jnp.mean(mixed32 * mixed32, axis=-1, keepdims=True) + 1e-06)
    normed = (mixed32 * scale * norm_gain).astype(jnp.bfloat16)
    all_rows = lax.all_gather(normed, "tp", axis=0, tiled=True)
    before = jnp.dot(
        all_rows,
        lax.all_gather(up_weight, "sp", axis=0, tiled=True),
        preferred_element_type=jnp.float32,
    )
    hidden = jnp.square(jax.nn.relu(before)).astype(jnp.bfloat16)
    terms = jnp.dot(
        hidden,
        lax.all_gather(down_weight, "sp", axis=1, tiled=True),
        preferred_element_type=jnp.float32,
    )
    down = lax.psum_scatter(
        terms.astype(jnp.bfloat16), "tp", scatter_dimension=0, tiled=True
    ).astype(jnp.float32)
    return (mixed32 + down).astype(jnp.bfloat16)


CHUNKS = 4
LEAD = 4
F32 = jnp.float32
BF16 = jnp.bfloat16


def remote(src, dst, send_sem, recv_sem, device_id):
    return pltpu.make_async_remote_copy(
        src_ref=src,
        dst_ref=dst,
        send_sem=send_sem,
        recv_sem=recv_sem,
        device_id=device_id,
        device_id_type=pl.DeviceIdType.MESH,
    )


def aligned(value, size):
    return pl.multiple_of(value * size, size)


def layer_kernel(
    n,
    queries,
    keys,
    values,
    sink,
    out_weight,
    residual,
    gain,
    up,
    down,
    out,
    q_buf,
    k_buf,
    v_buf,
    k_wide,
    v_wide,
    attended,
    att_all,
    ow_buf,
    res_buf,
    mixed,
    normed,
    up_buf,
    down_buf,
    acc,
    hidden,
    terms,
    pair_in,
    chip_sum,
    peer_in,
    local_sem,
    tail_send,
    tail_recv,
    z_send,
    y_send,
    w_recv,
    att_send,
    att_recv,
    norm_send,
    norm_recv,
    pair_send,
    pair_recv,
    peer_send,
    peer_recv,
):
    z = lax.axis_index("sp")
    y = lax.axis_index("grp")
    me = lax.axis_index("tp")
    partner = me + 1 - 2 * lax.rem(me, 2)
    across = lax.rem(me + 2, 4)
    diagonal = lax.rem(partner + 2, 4)
    rows, head_cols = q_buf.shape
    own = rows // 4
    depth = up.shape[0]
    width = down.shape[1]
    cols = up.shape[1]
    wide = n * width
    part = width // 2
    chunk = (depth // 2 // CHUNKS, down.shape[0] // 2 // (CHUNKS // 2))

    barrier = pltpu.get_barrier_semaphore()
    for step in range(1, 4):
        pl.semaphore_signal(
            barrier,
            inc=1,
            device_id={"tp": lax.rem(me + step, 4)},
            device_id_type=pl.DeviceIdType.MESH,
        )
    pl.semaphore_signal(
        barrier, inc=1, device_id={"grp": 1 - y}, device_id_type=pl.DeviceIdType.MESH
    )

    @pl.when(z > 0)
    def _():
        pl.semaphore_signal(
            barrier, inc=1, device_id={"sp": z - 1}, device_id_type=pl.DeviceIdType.MESH
        )

    @pl.when(z < n - 1)
    def _():
        pl.semaphore_signal(
            barrier, inc=1, device_id={"sp": z + 1}, device_id_type=pl.DeviceIdType.MESH
        )

    own_up = up_buf.at[pl.ds(aligned(z, depth), depth), :]
    locals_ = [
        pltpu.make_async_copy(keys, k_buf.at[:, pl.ds(WINDOW, rows)], local_sem.at[0]),
        pltpu.make_async_copy(values, v_buf.at[:, pl.ds(WINDOW, rows)], local_sem.at[1]),
        pltpu.make_async_copy(queries, q_buf, local_sem.at[2]),
        pltpu.make_async_copy(out_weight, ow_buf, local_sem.at[3]),
        pltpu.make_async_copy(residual, res_buf, local_sem.at[4]),
        pltpu.make_async_copy(up, own_up, local_sem.at[5]),
        pltpu.make_async_copy(down.at[:, pl.ds(0, part)], down_buf.at[z, 0], local_sem.at[6]),
        pltpu.make_async_copy(down.at[:, pl.ds(part, part)], down_buf.at[z, 1], local_sem.at[7]),
    ]
    for copy in locals_:
        copy.start()

    edge = jnp.where(z > 0, 1, 0) + jnp.where(z < n - 1, 1, 0)
    pl.semaphore_wait(barrier, 4 + edge)

    def piece(weight, owner, half, index):
        if weight == 0:
            start = owner * depth + half * (depth // 2) + index * chunk[0]
            return up_buf.at[pl.ds(pl.multiple_of(start, chunk[0]), chunk[0]), :]
        start = half * (2 * chunk[1]) + (index % 2) * chunk[1]
        return down_buf.at[
            owner, index // 2, pl.ds(pl.multiple_of(start, chunk[1]), chunk[1]), :
        ]

    def own_piece(weight, index):
        if weight == 0:
            start = y * (CHUNKS * chunk[0]) + index * chunk[0]
            return up.at[pl.ds(pl.multiple_of(start, chunk[0]), chunk[0]), :]
        start = y * (2 * chunk[1]) + (index % 2) * chunk[1]
        return down.at[
            pl.ds(pl.multiple_of(start, chunk[1]), chunk[1]),
            pl.ds(index // 2 * (width // 2), width // 2),
        ]

    def z_copy(weight, owner, index, upward, source=None):
        place = piece(weight, owner, y, index)
        return remote(
            place if source is None else source,
            place,
            z_send.at[upward, weight, owner, index],
            w_recv.at[weight, owner, y, index],
            {"sp": z + (1 if upward else -1)},
        )

    def y_copy(weight, owner, index):
        place = piece(weight, owner, y, index)
        return remote(
            place,
            place,
            y_send.at[weight, owner, index],
            w_recv.at[weight, owner, y, index],
            {"grp": 1 - y},
        )

    def wait_piece(weight, owner, half, index):
        place = piece(weight, owner, half, index)
        remote(
            place,
            place,
            y_send.at[weight, owner, index],
            w_recv.at[weight, owner, half, index],
            {"grp": 1 - y},
        ).wait_recv()

    def send_own(weight, upward):
        for index in range(CHUNKS):
            z_copy(weight, z, index, upward, own_piece(weight, index)).start()

    def tail_copy(which):
        source, place = ((keys, k_buf), (values, v_buf))[which]
        return remote(
            source.at[:, pl.ds(rows - WINDOW, WINDOW)],
            place.at[:, pl.ds(0, WINDOW)],
            tail_send.at[which],
            tail_recv.at[which],
            {"sp": z + 1},
        )

    @pl.when(z < n - 1)
    def _():
        tail_copy(0).start()
        tail_copy(1).start()
        send_own(0, 1)

    @pl.when(z > 0)
    def _():
        send_own(0, 0)

    def send_down(stage):
        @pl.when((z == stage) & (z < n - 1))
        def _():
            send_own(1, 1)

        @pl.when((n - 1 - z == stage) & (z > 0))
        def _():
            send_own(1, 0)

    send_down(0)

    near = jnp.minimum(z, n - 1 - z)
    far_sign = jnp.where(z < n - 1 - z, 1, -1)

    def owner_at(order):
        close = order <= 2 * near
        side = 2 * lax.rem(order + 1, 2) - 1
        return z + jnp.where(close, side * ((order + 1) // 2), far_sign * (order - near))

    def shard_at(number):
        span = 2 * CHUNKS
        close = number < near * span
        rest = number - near * span
        side = 2 * (number % 2) - 1
        owner = z + jnp.where(
            close,
            side * (number // span + 1),
            far_sign * (near + 1 + lax.div(jnp.maximum(rest, 0), CHUNKS)),
        )
        index = jnp.where(
            close, (number % span) // 2, lax.rem(jnp.maximum(rest, 0), CHUNKS)
        )
        return owner, index

    def event(weight, number):
        owner, index = shard_at(number)
        wait_piece(weight, owner, y, index)

        @pl.when((owner < z) & (z < n - 1))
        def _():
            z_copy(weight, owner, index, 1).start()

        @pl.when((owner > z) & (z > 0))
        def _():
            z_copy(weight, owner, index, 0).start()

        y_copy(weight, owner, index).start()

    total_events = (n - 1) * CHUNKS
    done = [0]
    halves = [0]

    def pump(until):
        while done[0] < min(until, 2 * total_events):
            weight, number = divmod(done[0], total_events)
            event(weight, number)
            done[0] += 1
            for stage in range(1, n - 1):
                if done[0] == min(stage * 2 * CHUNKS, total_events):
                    send_down(stage)

    def take_halves(until):
        while halves[0] < until:
            pump(halves[0] + 1 + LEAD)
            weight, number = divmod(halves[0], total_events)
            owner, index = shard_at(number)
            wait_piece(weight, owner, 1 - y, index)
            halves[0] += 1

    @pl.when(z == 0)
    def _():
        k_buf[:, pl.ds(0, WINDOW)] = jnp.zeros((HEAD_DIM, WINDOW), BF16)
        v_buf[:, pl.ds(0, WINDOW)] = jnp.zeros((HEAD_DIM, WINDOW), BF16)

    for copy in locals_[:3]:
        copy.wait()

    @pl.when(z > 0)
    def _():
        tail_copy(0).wait_recv()
        tail_copy(1).wait_recv()

    heads = head_cols // HEAD_DIM
    for h in range(heads):
        k_wide[h * HEAD_DIM : (h + 1) * HEAD_DIM, :] = k_buf[...]
        v_wide[h * HEAD_DIM : (h + 1) * HEAD_DIM, :] = v_buf[...]

    def attend(block, carry):
        start = aligned(block, WINDOW)
        q_rows = q_buf[pl.ds(start, WINDOW), :].astype(F32)
        lane_head = lax.broadcasted_iota(jnp.int32, (WINDOW, head_cols), 1) // HEAD_DIM
        stacked = jnp.concatenate(
            [jnp.where(lane_head == h, q_rows, 0.0) for h in range(heads)], axis=0
        ).astype(BF16)
        scores = jnp.dot(
            stacked, k_wide[:, pl.ds(start, 2 * WINDOW)], preferred_element_type=F32
        ) * HEAD_DIM ** (-0.5)
        i = lax.broadcasted_iota(jnp.int32, (heads * WINDOW, 2 * WINDOW), 0) % WINDOW
        j = lax.broadcasted_iota(jnp.int32, (heads * WINDOW, 2 * WINDOW), 1)
        first = WINDOW - z * rows - block * WINDOW
        valid = (j > i) & (j <= i + WINDOW) & (j >= first)
        scores = jnp.where(valid, scores, -1e30)
        sinks = jnp.concatenate(
            [jnp.full((WINDOW, 1), sink[h], F32) for h in range(heads)], axis=0
        )
        top = jnp.maximum(jnp.max(scores, axis=-1, keepdims=True), sinks)
        weights = jnp.exp(scores - top)
        total = jnp.sum(weights, axis=-1, keepdims=True) + jnp.exp(sinks - top)
        probs = (weights / total).astype(BF16)
        mixed_heads = lax.dot_general(
            probs,
            v_wide[:, pl.ds(start, 2 * WINDOW)],
            (((1,), (1,)), ((), ())),
            preferred_element_type=F32,
        )
        result = jnp.zeros((WINDOW, head_cols), F32)
        for h in range(heads):
            result += jnp.where(
                lane_head == h, mixed_heads[h * WINDOW : (h + 1) * WINDOW], 0.0
            )
        attended[pl.ds(start, WINDOW), :] = result.astype(BF16)
        return carry

    blocks = rows // WINDOW
    for block in range(0, blocks, 2):
        lax.fori_loop(block, min(block + 2, blocks), attend, 0)
        if block + 2 < blocks:
            pump(block // 2 + 1)

    def att_copy(step):
        peer = lax.rem(me + step, 4)
        return remote(
            attended.at[pl.ds(aligned(peer, own), own), :],
            att_all.at[me],
            att_send.at[step - 1],
            att_recv.at[me],
            {"tp": peer},
        )

    def att_wait(step):
        peer = lax.rem(me + step, 4)
        remote(
            att_all.at[peer], att_all.at[peer], att_send.at[step - 1], att_recv.at[peer], {"tp": peer}
        ).wait_recv()

    for step in (2, 1, 3):
        att_copy(step).start()
    att_all[me] = attended[pl.ds(aligned(me, own), own), :]
    pump(4)
    locals_[3].wait()
    locals_[4].wait()
    for step in (1, 2, 3):
        att_wait(step)

    tile = 256

    def project(index, squares):
        span = pl.ds(aligned(index, tile), tile)
        value = res_buf[:, span].astype(F32)
        for peer in range(4):
            value += jnp.dot(
                att_all[peer],
                ow_buf[peer * head_cols : (peer + 1) * head_cols, span],
                preferred_element_type=F32,
            )
        value = value.astype(BF16).astype(F32)
        mixed[:, span] = value
        return squares + jnp.sum(value * value, axis=-1, keepdims=True)

    squares = lax.fori_loop(0, wide // tile, project, jnp.zeros((own, 1), F32))
    scale = lax.rsqrt(squares / wide + 1e-06)
    own_rows = pl.ds(aligned(me, own), own)

    def normalize(index, carry):
        span = pl.ds(aligned(index, tile), tile)
        normed[own_rows, span] = (mixed[:, span] * scale * gain[:, span]).astype(BF16)
        return carry

    lax.fori_loop(0, wide // tile, normalize, 0)

    def norm_copy(slot, source, target):
        place = normed.at[pl.ds(aligned(source, own), own), :]
        return remote(place, place, norm_send.at[slot], norm_recv.at[source], {"tp": target})

    norm_copy(0, me, across).start()
    norm_copy(1, me, partner).start()
    pump(total_events + 2)
    norm_copy(2, across, across).wait_recv()
    norm_copy(2, across, partner).start()

    locals_[5].wait()
    norm_copy(2, partner, partner).wait_recv()
    norm_copy(2, diagonal, partner).wait_recv()

    for order in range(n):
        owner = owner_at(order) if order else z
        if order:
            take_halves(min(order + order % 2, n - 1) * CHUNKS)

        def up_step(index, carry, owner=owner, order=order):
            span = pl.ds(aligned(index, tile), tile)
            value = jnp.dot(
                normed[:, pl.ds(aligned(owner, depth), depth)],
                up_buf[pl.ds(aligned(owner, depth), depth), span],
                preferred_element_type=F32,
            )
            if order:
                value += acc[:, span]
            if order == n - 1:
                hidden[:, span] = jnp.square(jnp.maximum(value, 0.0)).astype(BF16)
            else:
                acc[:, span] = value
            return carry

        lax.fori_loop(0, cols // tile, up_step, 0)

    pieces = [(order, slice(0, width)) for order in range(n - 1)]
    pieces += [(n - 1, slice(0, part)), (n - 1, slice(part, width))]

    def pair_copy(which, slot):
        order, span = pieces[which]
        group = (partner, diagonal)[slot]
        return remote(
            terms.at[order, pl.ds(aligned(group, own), own), span],
            pair_in.at[order, slot, :, span],
            pair_send.at[which, slot],
            pair_recv.at[which, slot],
            {"tp": partner},
        )

    def peer_copy(which):
        order, span = pieces[which]
        return remote(
            chip_sum.at[order, :, span],
            peer_in.at[order, :, span],
            peer_send.at[which],
            peer_recv.at[which],
            {"tp": across},
        )

    def finish(which):
        order, span = pieces[which]
        owner = owner_at(order) if order else z
        size = span.stop - span.start
        target = pl.ds(pl.multiple_of(owner * width + span.start, size), size)
        peer_copy(which).wait_recv()
        pair_copy(which, 0).wait_recv()
        total = (
            terms[order, own_rows, span].astype(F32)
            + pair_in[order, 0, :, span].astype(F32)
            + peer_in[order, :, span].astype(F32)
        )
        out[:, target] = (mixed[:, target] + total).astype(BF16)

    locals_[6].wait()
    locals_[7].wait()
    for which, (order, span) in enumerate(pieces):
        owner = owner_at(order) if order else z
        if order:
            whole = min(order + order % 2, n - 1) * CHUNKS
            last = order == n - 1 and span.stop < width
            take_halves(total_events + whole - (CHUNKS // 2 if last and n % 2 == 0 else 0))
        for index in range(span.start // part, span.stop // part):
            terms[order, :, index * part : (index + 1) * part] = jnp.dot(
                hidden[...], down_buf[owner, index], preferred_element_type=F32
            ).astype(BF16)
        pair_copy(which, 1).start()
        pair_copy(which, 0).start()
        pair_copy(which, 1).wait_recv()
        other = pl.ds(aligned(across, own), own)
        chip_sum[order, :, span] = (
            terms[order, other, span].astype(F32) + pair_in[order, 1, :, span].astype(F32)
        ).astype(BF16)
        peer_copy(which).start()
        if which:
            finish(which - 1)
    finish(len(pieces) - 1)

    for step in (1, 2, 3):
        att_copy(step).wait_send()
    norm_copy(0, me, across).wait_send()
    norm_copy(1, me, partner).wait_send()
    norm_copy(2, across, partner).wait_send()
    for which in range(len(pieces)):
        pair_copy(which, 0).wait_send()
        pair_copy(which, 1).wait_send()
        peer_copy(which).wait_send()

    @pl.when(z < n - 1)
    def _():
        tail_copy(0).wait_send()
        tail_copy(1).wait_send()

    for weight in range(2):
        for owner in range(n):

            @pl.when((z >= owner) & (z < n - 1))
            def _():
                for index in range(CHUNKS):
                    z_copy(weight, owner, index, 1).wait_send()

            @pl.when((z <= owner) & (z > 0))
            def _():
                for index in range(CHUNKS):
                    z_copy(weight, owner, index, 0).wait_send()

            @pl.when(z != owner)
            def _():
                for index in range(CHUNKS):
                    y_copy(weight, owner, index).wait_send()


def fused_body(
    n,
    queries,
    key_rows,
    value_rows,
    sink_logits,
    out_weight,
    residual,
    norm_gain,
    up_weight,
    down_weight,
):
    rows, head_cols = queries.shape
    own, wide = residual.shape
    depth, cols = up_weight.shape
    width = down_weight.shape[1]
    vmem = lambda *shape: pltpu.VMEM(shape, BF16)
    dma = lambda *shape: pltpu.SemaphoreType.DMA(shape)
    hbm = pl.BlockSpec(memory_space=pl.ANY)
    return pl.pallas_call(
        functools.partial(layer_kernel, n),
        out_shape=jax.ShapeDtypeStruct((own, wide), BF16),
        in_specs=[
            hbm,
            hbm,
            hbm,
            pl.BlockSpec(memory_space=pltpu.SMEM),
            hbm,
            hbm,
            pl.BlockSpec(memory_space=pltpu.VMEM),
            hbm,
            hbm,
        ],
        out_specs=pl.BlockSpec(memory_space=pltpu.VMEM),
        scratch_shapes=[
            vmem(rows, head_cols),
            vmem(HEAD_DIM, rows + WINDOW),
            vmem(HEAD_DIM, rows + WINDOW),
            vmem(head_cols, rows + WINDOW),
            vmem(head_cols, rows + WINDOW),
            vmem(rows, head_cols),
            vmem(4, own, head_cols),
            vmem(*out_weight.shape),
            vmem(own, wide),
            pltpu.VMEM((own, wide), F32),
            vmem(rows, wide),
            vmem(n * depth, cols),
            vmem(n, 2, cols, width // 2),
            pltpu.VMEM((rows, cols), F32),
            vmem(rows, cols),
            vmem(n, rows, width),
            vmem(n, 2, own, width),
            vmem(n, own, width),
            vmem(n, own, width),
            dma(8),
            dma(2),
            dma(2),
            dma(2, 2, n, CHUNKS),
            dma(2, n, CHUNKS),
            dma(2, n, 2, CHUNKS),
            dma(3),
            dma(4),
            dma(3),
            dma(4),
            dma(n + 1, 2),
            dma(n + 1, 2),
            dma(n + 1),
            dma(n + 1),
        ],
        compiler_params=pltpu.CompilerParams(
            collective_id=0, has_side_effects=True, vmem_limit_bytes=60 * 1024 * 1024
        ),
    )(
        queries,
        key_rows.T,
        value_rows.T,
        sink_logits,
        out_weight,
        residual,
        norm_gain.reshape(1, -1),
        up_weight,
        down_weight,
    )


def solution(mesh):
    in_specs = (
        P(("grp", "sp"), "tp"),
        P(("grp", "sp"), "tp"),
        P(("grp", "sp"), "tp"),
        P("tp"),
        P(),
        P(("grp", "sp", "tp"), None),
        P(),
        P("sp", "tp"),
        P("tp", "sp"),
    )
    out_specs = P(("grp", "sp", "tp"), None)
    n = mesh.shape["sp"]
    shards_fit = 2 <= n <= 8

    def layer(*arrays):
        key_rows, up_weight, down_weight = arrays[1], arrays[7], arrays[8]
        fits = (
            shards_fit
            and mesh.shape["grp"] == 2
            and mesh.shape["tp"] == 4
            and key_rows.shape[1] == HEAD_DIM
            and up_weight.shape[0] % (32 * CHUNKS) == 0
            and up_weight.shape[1] % 256 == 0
            and down_weight.shape[1] % 256 == 0
        )
        return (functools.partial(fused_body, n) if fits else body)(*arrays)

    return jax.shard_map(layer, mesh=mesh, in_specs=in_specs, out_specs=out_specs, check_vma=False)
```

profile of v0, /device:TPU:0, one launch (start us, length us, event | category | flops | bytes accessed | tf_op | source)
XLA Modules:
  0.0 98.5 jit_solution(574465042941195124)
XLA Ops:
  0.0 96.5 %shard_map.91 = bf16[192,2048]{1,0:T(8,128)(2,1)} custom-call(bf16[768,256]{1,0:T(8,128)(2,1)} %queries.1, bf16[64,768]{1,0:T(8,128)(2,1)} %bitcast.3, bf16[64,768]{1,0:T(8,128)(2,1)} %bitcast.4, f32[4]{0:T(128)} %sink.1, bf16[1024,2048]{1,0:T(8,128)(2,1)} %out_weight.1, bf16[192,2048]{1,0:T(8,128)(2,1)} %residual.1, f32[1,2048]{1,0:T(1,128)} %bitcast.5, ...), custom_call_target="tpu_custom_call" | custom-call | tf_op jit(solution)/shard_map/pallas_call | solution.py:631
  96.5 2.1 %copy.11 = bf16[192,2048]{1,0:T(8,128)(2,1)} copy(bf16[192,2048]{1,0:T(8,128)(2,1)} %shard_map.91) | data formatting | bytes 1572864
where the time goes:
time: 98.8 us; the launch traced here: 98.5 us
  Pallas kernels  96.5 us (98%)
  local copies, waits for them, and re-layouts  2.09 us (2%)
    pallas_call x1, Pallas kernels, fused_body(): pl.pallas_call(functools.partial(layer_kernel, n), out_shape=jax.ShapeDty...  96.5 us
    unnamed x1, local copies, waits for them, and re-layouts  2.09 us

commit v1 on v0

--- a/solution.py
+++ b/solution.py
@@ -101,8 +101,9 @@
     return (mixed32 + down).astype(jnp.bfloat16)
 
 
-CHUNKS = 4
-LEAD = 4
+LEAD = 3
+PIECES = 2
+CHUNKS = 2 * PIECES
 F32 = jnp.float32
 BF16 = jnp.bfloat16
 
@@ -157,6 +158,7 @@
     tail_send,
     tail_recv,
     z_send,
+    twin_send,
     y_send,
     w_recv,
     att_send,
@@ -181,7 +183,11 @@
     cols = up.shape[1]
     wide = n * width
     part = width // 2
-    chunk = (depth // 2 // CHUNKS, down.shape[0] // 2 // (CHUNKS // 2))
+    lane = part // 2
+    chunk = (depth // 2 // CHUNKS, down.shape[0] // PIECES)
+    near = jnp.minimum(z, n - 1 - z)
+    is_end = near == 0
+    far_sign = jnp.where(z < n - 1 - z, 1, -1)
 
     barrier = pltpu.get_barrier_semaphore()
     for step in range(1, 4):
@@ -215,9 +221,11 @@
         pltpu.make_async_copy(out_weight, ow_buf, local_sem.at[3]),
         pltpu.make_async_copy(residual, res_buf, local_sem.at[4]),
         pltpu.make_async_copy(up, own_up, local_sem.at[5]),
-        pltpu.make_async_copy(down.at[:, pl.ds(0, part)], down_buf.at[z, 0], local_sem.at[6]),
-        pltpu.make_async_copy(down.at[:, pl.ds(part, part)], down_buf.at[z, 1], local_sem.at[7]),
     ]
+    for index in range(4):
+        source = down.at[:, pl.ds(index * lane, lane)]
+        place = down_buf.at[z, index // 2, index % 2]
+        locals_.append(pltpu.make_async_copy(source, place, local_sem.at[6 + index]))
     for copy in locals_:
         copy.start()
 
@@ -228,20 +236,15 @@
         if weight == 0:
             start = owner * depth + half * (depth // 2) + index * chunk[0]
             return up_buf.at[pl.ds(pl.multiple_of(start, chunk[0]), chunk[0]), :]
-        start = half * (2 * chunk[1]) + (index % 2) * chunk[1]
         return down_buf.at[
-            owner, index // 2, pl.ds(pl.multiple_of(start, chunk[1]), chunk[1]), :
+            owner, index // PIECES, half, pl.ds(aligned(index % PIECES, chunk[1]), chunk[1]), :
         ]
 
-    def own_piece(weight, index):
+    def own_piece(weight, half, index):
         if weight == 0:
-            start = y * (CHUNKS * chunk[0]) + index * chunk[0]
+            start = half * (depth // 2) + index * chunk[0]
             return up.at[pl.ds(pl.multiple_of(start, chunk[0]), chunk[0]), :]
-        start = y * (2 * chunk[1]) + (index % 2) * chunk[1]
-        return down.at[
-            pl.ds(pl.multiple_of(start, chunk[1]), chunk[1]),
-            pl.ds(index // 2 * (width // 2), width // 2),
-        ]
+        return piece(weight, z, half, index)
 
     def z_copy(weight, owner, index, upward, source=None):
         place = piece(weight, owner, y, index)
@@ -253,6 +256,15 @@
             {"sp": z + (1 if upward else -1)},
         )
 
+    def twin_copy(weight, index):
+        return remote(
+            own_piece(weight, 1 - y, index),
+            piece(weight, z, 1 - y, index),
+            twin_send.at[weight, index],
+            w_recv.at[weight, z, 1 - y, index],
+            {"sp": z + far_sign},
+        )
+
     def y_copy(weight, owner, index):
         place = piece(weight, owner, y, index)
         return remote(
@@ -262,6 +274,9 @@
             w_recv.at[weight, owner, y, index],
             {"grp": 1 - y},
         )
+
+    def has_twin(owner):
+        return ((z == 1) & (owner == 0)) | ((z == n - 2) & (owner == n - 1))
 
     def wait_piece(weight, owner, half, index):
         place = piece(weight, owner, half, index)
@@ -273,9 +288,15 @@
             {"grp": 1 - y},
         ).wait_recv()
 
+    def each_piece(action):
+        def step(index, carry):
+            action(index)
+            return carry
+
+        lax.fori_loop(0, CHUNKS, step, 0)
+
     def send_own(weight, upward):
-        for index in range(CHUNKS):
-            z_copy(weight, z, index, upward, own_piece(weight, index)).start()
+        each_piece(lambda index: z_copy(weight, z, index, upward, own_piece(weight, y, index)).start())
 
     def tail_copy(which):
         source, place = ((keys, k_buf), (values, v_buf))[which]
@@ -297,39 +318,27 @@
     def _():
         send_own(0, 0)
 
-    def send_down(stage):
-        @pl.when((z == stage) & (z < n - 1))
-        def _():
-            send_own(1, 1)
-
-        @pl.when((n - 1 - z == stage) & (z > 0))
-        def _():
-            send_own(1, 0)
-
-    send_down(0)
-
-    near = jnp.minimum(z, n - 1 - z)
-    far_sign = jnp.where(z < n - 1 - z, 1, -1)
+    @pl.when(is_end)
+    def _():
+        each_piece(lambda index: twin_copy(0, index).start())
 
     def owner_at(order):
         close = order <= 2 * near
         side = 2 * lax.rem(order + 1, 2) - 1
         return z + jnp.where(close, side * ((order + 1) // 2), far_sign * (order - near))
 
+    def unit_at(unit):
+        close = unit < near * 4
+        rest = jnp.maximum(unit - near * 4, 0)
+        side = 2 * (unit % 2) - 1
+        owner = z + jnp.where(
+            close, side * (unit // 4 + 1), far_sign * (near + 1 + lax.div(rest, 2))
+        )
+        return owner, jnp.where(close, (unit % 4) // 2, lax.rem(rest, 2))
+
     def shard_at(number):
-        span = 2 * CHUNKS
-        close = number < near * span
-        rest = number - near * span
-        side = 2 * (number % 2) - 1
-        owner = z + jnp.where(
-            close,
-            side * (number // span + 1),
-            far_sign * (near + 1 + lax.div(jnp.maximum(rest, 0), CHUNKS)),
-        )
-        index = jnp.where(
-            close, (number % span) // 2, lax.rem(jnp.maximum(rest, 0), CHUNKS)
-        )
-        return owner, index
+        owner, block = unit_at(number // PIECES)
+        return owner, block * PIECES + number % PIECES
 
     def event(weight, number):
         owner, index = shard_at(number)
@@ -343,36 +352,76 @@
         def _():
             z_copy(weight, owner, index, 0).start()
 
-        y_copy(weight, owner, index).start()
-
-    total_events = (n - 1) * CHUNKS
-    done = [0]
-    halves = [0]
-
-    def pump(until):
-        while done[0] < min(until, 2 * total_events):
-            weight, number = divmod(done[0], total_events)
-            event(weight, number)
-            done[0] += 1
-            for stage in range(1, n - 1):
-                if done[0] == min(stage * 2 * CHUNKS, total_events):
-                    send_down(stage)
-
-    def take_halves(until):
-        while halves[0] < until:
-            pump(halves[0] + 1 + LEAD)
-            weight, number = divmod(halves[0], total_events)
-            owner, index = shard_at(number)
-            wait_piece(weight, owner, 1 - y, index)
-            halves[0] += 1
+        @pl.when(jnp.logical_not(has_twin(owner)))
+        def _():
+            y_copy(weight, owner, index).start()
+
+    total = (n - 1) * CHUNKS
+
+    def pick(end, middle):
+        return end if end == middle else jnp.where(is_end, end, middle)
+
+    def run(action, weight, state, goals):
+        starts = [min(max(at - weight * total, 0), total) for at in state]
+        stops = [min(max(at - weight * total, 0), total) for at in goals]
+        if starts == stops:
+            return
+
+        def step(number, carry):
+            action(weight, number)
+            return carry
+
+        lax.fori_loop(pick(*starts), pick(*stops), step, 0)
+
+    arrived = [0, 0]
+    halves = [0, 0]
+
+    def scaled(count):
+        return min(count * CHUNKS // 4, 2 * total)
+
+    def advance(end, middle):
+        goals = [max(arrived[0], scaled(end)), max(arrived[1], scaled(middle))]
+        run(event, 0, arrived, goals)
+        if arrived[1] < total <= goals[1]:
+
+            @pl.when(jnp.logical_not(is_end))
+            def _():
+                send_own(1, 1)
+                send_own(1, 0)
+
+        run(event, 1, arrived, goals)
+        arrived[:] = goals
+
+    def take_half(weight, number):
+        owner, index = shard_at(number)
+        wait_piece(weight, owner, 1 - y, index)
+
+    def take(end, middle):
+        goals = [max(halves[0], scaled(end)), max(halves[1], scaled(middle))]
+        assert goals[0] <= arrived[0] and goals[1] <= arrived[1]
+        run(take_half, 0, halves, goals)
+        run(take_half, 1, halves, goals)
+        halves[:] = goals
 
     @pl.when(z == 0)
     def _():
         k_buf[:, pl.ds(0, WINDOW)] = jnp.zeros((HEAD_DIM, WINDOW), BF16)
         v_buf[:, pl.ds(0, WINDOW)] = jnp.zeros((HEAD_DIM, WINDOW), BF16)
 
-    for copy in locals_[:3]:
+    for copy in (*locals_[:3], *locals_[6:]):
         copy.wait()
+
+    @pl.when(is_end)
+    def _():
+        @pl.when(z < n - 1)
+        def _():
+            send_own(1, 1)
+
+        @pl.when(z > 0)
+        def _():
+            send_own(1, 0)
+
+        each_piece(lambda index: twin_copy(1, index).start())
 
     @pl.when(z > 0)
     def _():
@@ -423,8 +472,7 @@
     blocks = rows // WINDOW
     for block in range(0, blocks, 2):
         lax.fori_loop(block, min(block + 2, blocks), attend, 0)
-        if block + 2 < blocks:
-            pump(block // 2 + 1)
+        advance((0, 1, 3)[min(block // 2, 2)], (0, 4, 6)[min(block // 2, 2)])
 
     def att_copy(step):
         peer = lax.rem(me + step, 4)
@@ -445,11 +493,12 @@
     for step in (2, 1, 3):
         att_copy(step).start()
     att_all[me] = attended[pl.ds(aligned(me, own), own), :]
-    pump(4)
+    advance(4, 8)
     locals_[3].wait()
     locals_[4].wait()
     for step in (1, 2, 3):
         att_wait(step)
+    advance(5, 9)
 
     tile = 256
 
@@ -470,31 +519,32 @@
     scale = lax.rsqrt(squares / wide + 1e-06)
     own_rows = pl.ds(aligned(me, own), own)
 
-    def normalize(index, carry):
-        span = pl.ds(aligned(index, tile), tile)
+    def norm_copy(slot, order, source, target):
+        place = normed.at[
+            pl.ds(aligned(source, own), own), pl.ds(aligned(owner_at(order), depth), depth)
+        ]
+        return remote(
+            place, place, norm_send.at[order, slot], norm_recv.at[order, source], {"tp": target}
+        )
+
+    for order in range(n):
+        span = pl.ds(aligned(owner_at(order), depth), depth)
         normed[own_rows, span] = (mixed[:, span] * scale * gain[:, span]).astype(BF16)
-        return carry
-
-    lax.fori_loop(0, wide // tile, normalize, 0)
-
-    def norm_copy(slot, source, target):
-        place = normed.at[pl.ds(aligned(source, own), own), :]
-        return remote(place, place, norm_send.at[slot], norm_recv.at[source], {"tp": target})
-
-    norm_copy(0, me, across).start()
-    norm_copy(1, me, partner).start()
-    pump(total_events + 2)
-    norm_copy(2, across, across).wait_recv()
-    norm_copy(2, across, partner).start()
+        norm_copy(0, order, me, across).start()
+        norm_copy(1, order, me, partner).start()
 
     locals_[5].wait()
-    norm_copy(2, partner, partner).wait_recv()
-    norm_copy(2, diagonal, partner).wait_recv()
-
+    plan = ((7, 11), (10, 13), (11, 16), (13, 19))
     for order in range(n):
-        owner = owner_at(order) if order else z
-        if order:
-            take_halves(min(order + order % 2, n - 1) * CHUNKS)
+        owner = owner_at(order)
+        advance(*plan[order])
+        norm_copy(2, order, across, across).wait_recv()
+        norm_copy(2, order, across, partner).start()
+        if order != 1:
+            advance(*(count + 1 for count in plan[order]))
+        take(4 * order, 4 * min(order + order % 2, n - 1))
+        norm_copy(2, order, partner, partner).wait_recv()
+        norm_copy(2, order, diagonal, partner).wait_recv()
 
         def up_step(index, carry, owner=owner, order=order):
             span = pl.ds(aligned(index, tile), tile)
@@ -513,74 +563,97 @@
 
         lax.fori_loop(0, cols // tile, up_step, 0)
 
-    pieces = [(order, slice(0, width)) for order in range(n - 1)]
-    pieces += [(n - 1, slice(0, part)), (n - 1, slice(part, width))]
+    blocks = 2 * n
+    last = blocks - 1
+
+    def place_of(which):
+        if which < 2:
+            return z, which, 0, part
+        owner, block = unit_at(min(which, last) - 2)
+        if which < last:
+            return owner, block, 0, part
+        return owner, block, (y if which == last else 1 - y) * lane, lane
 
     def pair_copy(which, slot):
-        order, span = pieces[which]
+        size = place_of(which)[3]
         group = (partner, diagonal)[slot]
         return remote(
-            terms.at[order, pl.ds(aligned(group, own), own), span],
-            pair_in.at[order, slot, :, span],
+            terms.at[which, pl.ds(aligned(group, own), own), pl.ds(0, size)],
+            pair_in.at[which, slot, :, pl.ds(0, size)],
             pair_send.at[which, slot],
             pair_recv.at[which, slot],
             {"tp": partner},
         )
 
     def peer_copy(which):
-        order, span = pieces[which]
+        size = place_of(which)[3]
         return remote(
-            chip_sum.at[order, :, span],
-            peer_in.at[order, :, span],
+            chip_sum.at[which, :, pl.ds(0, size)],
+            peer_in.at[which, :, pl.ds(0, size)],
             peer_send.at[which],
             peer_recv.at[which],
             {"tp": across},
         )
 
+    def multiply(which):
+        owner, block, offset, size = place_of(which)
+        if size == part:
+            weight = jnp.concatenate([down_buf[owner, block, half] for half in range(2)], axis=1)
+        else:
+            weight = down_buf[owner, block, y if which == last else 1 - y]
+        terms[which, :, 0:size] = jnp.dot(
+            hidden[...], weight, preferred_element_type=F32
+        ).astype(BF16)
+        pair_copy(which, 1).start()
+        pair_copy(which, 0).start()
+
+    def combine(which):
+        size = place_of(which)[3]
+        pair_copy(which, 1).wait_recv()
+        other = pl.ds(aligned(across, own), own)
+        chip_sum[which, :, 0:size] = (
+            terms[which, other, 0:size].astype(F32) + pair_in[which, 1, :, 0:size].astype(F32)
+        ).astype(BF16)
+        peer_copy(which).start()
+
     def finish(which):
-        order, span = pieces[which]
-        owner = owner_at(order) if order else z
-        size = span.stop - span.start
-        target = pl.ds(pl.multiple_of(owner * width + span.start, size), size)
+        owner, block, offset, size = place_of(which)
+        target = pl.ds(pl.multiple_of(owner * width + block * part + offset, size), size)
         peer_copy(which).wait_recv()
         pair_copy(which, 0).wait_recv()
-        total = (
-            terms[order, own_rows, span].astype(F32)
-            + pair_in[order, 0, :, span].astype(F32)
-            + peer_in[order, :, span].astype(F32)
-        )
-        out[:, target] = (mixed[:, target] + total).astype(BF16)
-
-    locals_[6].wait()
-    locals_[7].wait()
-    for which, (order, span) in enumerate(pieces):
-        owner = owner_at(order) if order else z
-        if order:
-            whole = min(order + order % 2, n - 1) * CHUNKS
-            last = order == n - 1 and span.stop < width
-            take_halves(total_events + whole - (CHUNKS // 2 if last and n % 2 == 0 else 0))
-        for index in range(span.start // part, span.stop // part):
-            terms[order, :, index * part : (index + 1) * part] = jnp.dot(
-                hidden[...], down_buf[owner, index], preferred_element_type=F32
-            ).astype(BF16)
-        pair_copy(which, 1).start()
-        pair_copy(which, 0).start()
-        pair_copy(which, 1).wait_recv()
-        other = pl.ds(aligned(across, own), own)
-        chip_sum[order, :, span] = (
-            terms[order, other, span].astype(F32) + pair_in[order, 1, :, span].astype(F32)
-        ).astype(BF16)
-        peer_copy(which).start()
+        value = (
+            terms[which, own_rows, 0:size].astype(F32)
+            + pair_in[which, 0, :, 0:size].astype(F32)
+            + peer_in[which, :, 0:size].astype(F32)
+        )
+        out[:, target] = (mixed[:, target] + value).astype(BF16)
+
+    first = 4 * (n - 1)
+    for which in range(blocks + 1):
+        ready = first + 2 * (min(which, last) - 1)
+        if which < 2:
+            advance(first + 3 + which, first + 7 + which)
+        elif which != last:
+            for step in range(2):
+                advance(ready - 1 + step + LEAD, ready + 6)
+                take(ready - 1 + step, ready - 1 + step)
+        else:
+            advance(ready, ready + 6)
+        multiply(which)
+        combine(which)
+        if which == 1:
+            advance(first + 5, first + 9)
         if which:
             finish(which - 1)
-    finish(len(pieces) - 1)
+    finish(blocks)
 
     for step in (1, 2, 3):
         att_copy(step).wait_send()
-    norm_copy(0, me, across).wait_send()
-    norm_copy(1, me, partner).wait_send()
-    norm_copy(2, across, partner).wait_send()
-    for which in range(len(pieces)):
+    for order in range(n):
+        norm_copy(0, order, me, across).wait_send()
+        norm_copy(1, order, me, partner).wait_send()
+        norm_copy(2, order, across, partner).wait_send()
+    for which in range(blocks + 1):
         pair_copy(which, 0).wait_send()
         pair_copy(which, 1).wait_send()
         peer_copy(which).wait_send()
@@ -591,22 +664,24 @@
         tail_copy(1).wait_send()
 
     for weight in range(2):
+
+        @pl.when(is_end)
+        def _():
+            each_piece(lambda index: twin_copy(weight, index).wait_send())
+
         for owner in range(n):
 
             @pl.when((z >= owner) & (z < n - 1))
             def _():
-                for index in range(CHUNKS):
-                    z_copy(weight, owner, index, 1).wait_send()
+                each_piece(lambda index: z_copy(weight, owner, index, 1).wait_send())
 
             @pl.when((z <= owner) & (z > 0))
             def _():
-                for index in range(CHUNKS):
-                    z_copy(weight, owner, index, 0).wait_send()
-
-            @pl.when(z != owner)
+                each_piece(lambda index: z_copy(weight, owner, index, 0).wait_send())
+
+            @pl.when((z != owner) & jnp.logical_not(has_twin(owner)))
             def _():
-                for index in range(CHUNKS):
-                    y_copy(weight, owner, index).wait_send()
+                each_piece(lambda index: y_copy(weight, owner, index).wait_send())
 
 
 def fused_body(
@@ -625,12 +700,13 @@
     own, wide = residual.shape
     depth, cols = up_weight.shape
     width = down_weight.shape[1]
+    part = width // 2
     vmem = lambda *shape: pltpu.VMEM(shape, BF16)
     dma = lambda *shape: pltpu.SemaphoreType.DMA(shape)
     hbm = pl.BlockSpec(memory_space=pl.ANY)
     return pl.pallas_call(
         functools.partial(layer_kernel, n),
-        out_shape=jax.ShapeDtypeStruct((own, wide), BF16),
+        out_shape=pltpu.VMEM((own, wide), BF16),
         in_specs=[
             hbm,
             hbm,
@@ -656,27 +732,28 @@
             pltpu.VMEM((own, wide), F32),
             vmem(rows, wide),
             vmem(n * depth, cols),
-            vmem(n, 2, cols, width // 2),
+            vmem(n, 2, 2, cols, part // 2),
             pltpu.VMEM((rows, cols), F32),
             vmem(rows, cols),
-            vmem(n, rows, width),
-            vmem(n, 2, own, width),
-            vmem(n, own, width),
-            vmem(n, own, width),
-            dma(8),
+            vmem(2 * n + 1, rows, part),
+            vmem(2 * n + 1, 2, own, part),
+            vmem(2 * n + 1, own, part),
+            vmem(2 * n + 1, own, part),
+            dma(10),
             dma(2),
             dma(2),
             dma(2, 2, n, CHUNKS),
+            dma(2, CHUNKS),
             dma(2, n, CHUNKS),
             dma(2, n, 2, CHUNKS),
             dma(3),
             dma(4),
-            dma(3),
-            dma(4),
-            dma(n + 1, 2),
-            dma(n + 1, 2),
-            dma(n + 1),
-            dma(n + 1),
+            dma(n, 3),
+            dma(n, 4),
+            dma(2 * n + 1, 2),
+            dma(2 * n + 1, 2),
+            dma(2 * n + 1),
+            dma(2 * n + 1),
         ],
         compiler_params=pltpu.CompilerParams(
             collective_id=0, has_side_effects=True, vmem_limit_bytes=60 * 1024 * 1024
@@ -708,18 +785,17 @@
     )
     out_specs = P(("grp", "sp", "tp"), None)
     n = mesh.shape["sp"]
-    shards_fit = 2 <= n <= 8
 
     def layer(*arrays):
         key_rows, up_weight, down_weight = arrays[1], arrays[7], arrays[8]
         fits = (
-            shards_fit
+            n == 4
             and mesh.shape["grp"] == 2
             and mesh.shape["tp"] == 4
             and key_rows.shape[1] == HEAD_DIM
             and up_weight.shape[0] % (32 * CHUNKS) == 0
             and up_weight.shape[1] % 256 == 0
-            and down_weight.shape[1] % 256 == 0
+            and down_weight.shape[1] % 512 == 0
         )
         return (functools.partial(fused_body, n) if fits else body)(*arrays)
 

time: 98.8 us -> 90.3 us (0.914)
  Pallas kernels: 96.5 us -> 89.2 us
  local copies, waits for them, and re-layouts: 2.09 us -> 0.88 us
    pallas_call x1, Pallas kernels: 96.5 us -> 89.2 us  [fused_body(): pl.pallas_call(functools.partial(layer_kernel, n), out_shape=pltpu.VMEM((...]
    unnamed x1, local copies, waits for them, and re-layouts: 2.09 us -> 0.88 us
where the time goes in v1:
time: 90.3 us; the launch traced here: 90 us
  Pallas kernels  89.2 us (99%)
    pallas_call x1, Pallas kernels, fused_body(): pl.pallas_call(functools.partial(layer_kernel, n), out_shape=pltpu.VMEM((...  89.2 us

profile of v1, /device:TPU:0, one launch (start us, length us, event | category | flops | bytes accessed | tf_op | source)
XLA Modules:
  0.0 90.0 jit_solution(5253491264678163684)
XLA Ops:
  0.0 89.2 %shard_map.91 = bf16[192,2048]{1,0:T(8,128)(2,1)S(1)} custom-call(bf16[768,256]{1,0:T(8,128)(2,1)} %queries.1, bf16[64,768]{1,0:T(8,128)(2,1)} %bitcast.3, bf16[64,768]{1,0:T(8,128)(2,1)} %bitcast.4, f32[4]{0:T(128)} %sink.1, bf16[1024,2048]{1,0:T(8,128)(2,1)} %out_weight.1, bf16[192,2048]{1,0:T(8,128)(2,1)} %residual.1, f32[1,2048]{1,0:T(1,128)} %bitcast.5, ...), custom_call_target="tpu_custom_call" | custom-call | tf_op jit(solution)/shard_map/pallas_call | solution.py:707
  89.2 0.9 copy.11

commit v2 on v1

--- a/solution.py
+++ b/solution.py
@@ -101,8 +101,9 @@
     return (mixed32 + down).astype(jnp.bfloat16)
 
 
-LEAD = 3
-PIECES = 2
+PIECES = 4
+HOP = 4.7
+PACE = 2.8
 CHUNKS = 2 * PIECES
 F32 = jnp.float32
 BF16 = jnp.bfloat16
@@ -128,16 +129,18 @@
     queries,
     keys,
     values,
-    sink,
+    sink_in,
     out_weight,
     residual,
-    gain,
+    gain_in,
     up,
     down,
     out,
+    sink,
+    gain,
+    out_buf,
     q_buf,
-    k_buf,
-    v_buf,
+    kv_buf,
     k_wide,
     v_wide,
     attended,
@@ -155,19 +158,18 @@
     chip_sum,
     peer_in,
     local_sem,
-    tail_send,
-    tail_recv,
+    tail_sem,
     z_send,
     twin_send,
     y_send,
-    w_recv,
-    att_send,
-    att_recv,
+    z_recv,
+    y_up,
+    y_down,
+    att_sem,
     norm_send,
     norm_recv,
-    pair_send,
+    send_sem,
     pair_recv,
-    peer_send,
     peer_recv,
 ):
     z = lax.axis_index("sp")
@@ -214,18 +216,21 @@
         )
 
     own_up = up_buf.at[pl.ds(aligned(z, depth), depth), :]
-    locals_ = [
-        pltpu.make_async_copy(keys, k_buf.at[:, pl.ds(WINDOW, rows)], local_sem.at[0]),
-        pltpu.make_async_copy(values, v_buf.at[:, pl.ds(WINDOW, rows)], local_sem.at[1]),
-        pltpu.make_async_copy(queries, q_buf, local_sem.at[2]),
-        pltpu.make_async_copy(out_weight, ow_buf, local_sem.at[3]),
-        pltpu.make_async_copy(residual, res_buf, local_sem.at[4]),
-        pltpu.make_async_copy(up, own_up, local_sem.at[5]),
-    ]
+    wait_of = lambda ref, sem: pltpu.make_async_copy(ref, ref, sem).wait()
+    pltpu.make_async_copy(keys, kv_buf.at[0, :, pl.ds(WINDOW, rows)], local_sem.at[0]).start()
+    pltpu.make_async_copy(values, kv_buf.at[1, :, pl.ds(WINDOW, rows)], local_sem.at[0]).start()
     for index in range(4):
         source = down.at[:, pl.ds(index * lane, lane)]
         place = down_buf.at[z, index // 2, index % 2]
-        locals_.append(pltpu.make_async_copy(source, place, local_sem.at[6 + index]))
+        pltpu.make_async_copy(source, place, local_sem.at[1]).start()
+    locals_ = [
+        pltpu.make_async_copy(queries, q_buf, local_sem.at[2]),
+        pltpu.make_async_copy(sink_in, sink, local_sem.at[3]),
+        pltpu.make_async_copy(out_weight, ow_buf, local_sem.at[4]),
+        pltpu.make_async_copy(residual, res_buf, local_sem.at[5]),
+        pltpu.make_async_copy(gain_in, gain, local_sem.at[6]),
+        pltpu.make_async_copy(up, own_up, local_sem.at[7]),
+    ]
     for copy in locals_:
         copy.start()
 
@@ -246,22 +251,40 @@
             return up.at[pl.ds(pl.multiple_of(start, chunk[0]), chunk[0]), :]
         return piece(weight, z, half, index)
 
+    def half_of(weight, owner, half):
+        if weight == 0:
+            start = owner * depth + half * (depth // 2)
+            return up_buf.at[pl.ds(pl.multiple_of(start, depth // 2), depth // 2), :]
+        return down_buf.at[owner, :, half]
+
+    def slot_of(owner, position):
+        return lax.rem(owner - position + n, n) - 1
+
+    def z_slot(owner, upward):
+        return owner if upward else jnp.where(owner == z, n, owner)
+
     def z_copy(weight, owner, index, upward, source=None):
         place = piece(weight, owner, y, index)
+        target = z + (1 if upward else -1)
         return remote(
             place if source is None else source,
             place,
-            z_send.at[upward, weight, owner, index],
-            w_recv.at[weight, owner, y, index],
-            {"sp": z + (1 if upward else -1)},
-        )
+            z_send.at[weight, z_slot(owner, upward)],
+            z_recv.at[weight, slot_of(owner, target), index],
+            {"sp": target},
+        )
+
+    def half_sem(weight, owner, position, index):
+        if weight == 0:
+            return y_up.at[slot_of(owner, position)]
+        return y_down.at[slot_of(owner, position), index // (PIECES // 2)]
 
     def twin_copy(weight, index):
         return remote(
             own_piece(weight, 1 - y, index),
             piece(weight, z, 1 - y, index),
-            twin_send.at[weight, index],
-            w_recv.at[weight, z, 1 - y, index],
+            twin_send.at[weight],
+            half_sem(weight, z, z + far_sign, index),
             {"sp": z + far_sign},
         )
 
@@ -270,23 +293,13 @@
         return remote(
             place,
             place,
-            y_send.at[weight, owner, index],
-            w_recv.at[weight, owner, y, index],
+            y_send.at[weight, slot_of(owner, z)],
+            half_sem(weight, owner, z, index),
             {"grp": 1 - y},
         )
 
     def has_twin(owner):
         return ((z == 1) & (owner == 0)) | ((z == n - 2) & (owner == n - 1))
-
-    def wait_piece(weight, owner, half, index):
-        place = piece(weight, owner, half, index)
-        remote(
-            place,
-            place,
-            y_send.at[weight, owner, index],
-            w_recv.at[weight, owner, half, index],
-            {"grp": 1 - y},
-        ).wait_recv()
 
     def each_piece(action):
         def step(index, carry):
@@ -299,12 +312,11 @@
         each_piece(lambda index: z_copy(weight, z, index, upward, own_piece(weight, y, index)).start())
 
     def tail_copy(which):
-        source, place = ((keys, k_buf), (values, v_buf))[which]
         return remote(
-            source.at[:, pl.ds(rows - WINDOW, WINDOW)],
-            place.at[:, pl.ds(0, WINDOW)],
-            tail_send.at[which],
-            tail_recv.at[which],
+            (keys, values)[which].at[:, pl.ds(rows - WINDOW, WINDOW)],
+            kv_buf.at[which, :, pl.ds(0, WINDOW)],
+            tail_sem.at[0],
+            tail_sem.at[1],
             {"sp": z + 1},
         )
 
@@ -342,7 +354,7 @@
 
     def event(weight, number):
         owner, index = shard_at(number)
-        wait_piece(weight, owner, y, index)
+        wait_of(piece(weight, owner, y, index), z_recv.at[weight, slot_of(owner, z), index])
 
         @pl.when((owner < z) & (z < n - 1))
         def _():
@@ -361,27 +373,23 @@
     def pick(end, middle):
         return end if end == middle else jnp.where(is_end, end, middle)
 
-    def run(action, weight, state, goals):
-        starts = [min(max(at - weight * total, 0), total) for at in state]
+    arrived = [0, 0]
+
+    def run(weight, goals):
+        starts = [min(max(at - weight * total, 0), total) for at in arrived]
         stops = [min(max(at - weight * total, 0), total) for at in goals]
         if starts == stops:
             return
 
         def step(number, carry):
-            action(weight, number)
+            event(weight, number)
             return carry
 
         lax.fori_loop(pick(*starts), pick(*stops), step, 0)
 
-    arrived = [0, 0]
-    halves = [0, 0]
-
-    def scaled(count):
-        return min(count * CHUNKS // 4, 2 * total)
-
     def advance(end, middle):
-        goals = [max(arrived[0], scaled(end)), max(arrived[1], scaled(middle))]
-        run(event, 0, arrived, goals)
+        goals = [max(arrived[0], min(end, 2 * total)), max(arrived[1], min(middle, 2 * total))]
+        run(0, goals)
         if arrived[1] < total <= goals[1]:
 
             @pl.when(jnp.logical_not(is_end))
@@ -389,26 +397,26 @@
                 send_own(1, 1)
                 send_own(1, 0)
 
-        run(event, 1, arrived, goals)
+        run(1, goals)
         arrived[:] = goals
 
-    def take_half(weight, number):
-        owner, index = shard_at(number)
-        wait_piece(weight, owner, 1 - y, index)
-
-    def take(end, middle):
-        goals = [max(halves[0], scaled(end)), max(halves[1], scaled(middle))]
-        assert goals[0] <= arrived[0] and goals[1] <= arrived[1]
-        run(take_half, 0, halves, goals)
-        run(take_half, 1, halves, goals)
-        halves[:] = goals
+    def forward(clock):
+        fine = PACE * 4 / CHUNKS
+        landed = lambda since: max(int((clock - HOP - since) // fine), 0)
+        middle = 0
+        for since in (0, 8 * PACE):
+            side = min(landed(since), CHUNKS)
+            middle += 2 * PIECES * (side // PIECES) + side % PIECES
+            middle += min(max(landed(since) - CHUNKS, 0), CHUNKS)
+        advance(landed(0), middle)
 
     @pl.when(z == 0)
     def _():
-        k_buf[:, pl.ds(0, WINDOW)] = jnp.zeros((HEAD_DIM, WINDOW), BF16)
-        v_buf[:, pl.ds(0, WINDOW)] = jnp.zeros((HEAD_DIM, WINDOW), BF16)
-
-    for copy in (*locals_[:3], *locals_[6:]):
+        kv_buf[:, :, pl.ds(0, WINDOW)] = jnp.zeros((2, HEAD_DIM, WINDOW), BF16)
+
+    wait_of(kv_buf.at[:, :, pl.ds(WINDOW, rows)], local_sem.at[0])
+    wait_of(down_buf.at[z], local_sem.at[1])
+    for copy in locals_[:2]:
         copy.wait()
 
     @pl.when(is_end)
@@ -425,13 +433,12 @@
 
     @pl.when(z > 0)
     def _():
-        tail_copy(0).wait_recv()
-        tail_copy(1).wait_recv()
+        wait_of(kv_buf.at[:, :, pl.ds(0, WINDOW)], tail_sem.at[1])
 
     heads = head_cols // HEAD_DIM
     for h in range(heads):
-        k_wide[h * HEAD_DIM : (h + 1) * HEAD_DIM, :] = k_buf[...]
-        v_wide[h * HEAD_DIM : (h + 1) * HEAD_DIM, :] = v_buf[...]
+        k_wide[h * HEAD_DIM : (h + 1) * HEAD_DIM, :] = kv_buf[0]
+        v_wide[h * HEAD_DIM : (h + 1) * HEAD_DIM, :] = kv_buf[1]
 
     def attend(block, carry):
         start = aligned(block, WINDOW)
@@ -470,35 +477,29 @@
         return carry
 
     blocks = rows // WINDOW
-    for block in range(0, blocks, 2):
-        lax.fori_loop(block, min(block + 2, blocks), attend, 0)
-        advance((0, 1, 3)[min(block // 2, 2)], (0, 4, 6)[min(block // 2, 2)])
+    for block in range(blocks):
+        lax.fori_loop(block, block + 1, attend, 0)
+        forward(5.5 + 1.35 * block)
 
     def att_copy(step):
         peer = lax.rem(me + step, 4)
         return remote(
             attended.at[pl.ds(aligned(peer, own), own), :],
             att_all.at[me],
-            att_send.at[step - 1],
-            att_recv.at[me],
+            att_sem.at[0],
+            att_sem.at[1],
             {"tp": peer},
         )
-
-    def att_wait(step):
-        peer = lax.rem(me + step, 4)
-        remote(
-            att_all.at[peer], att_all.at[peer], att_send.at[step - 1], att_recv.at[peer], {"tp": peer}
-        ).wait_recv()
 
     for step in (2, 1, 3):
         att_copy(step).start()
     att_all[me] = attended[pl.ds(aligned(me, own), own), :]
-    advance(4, 8)
-    locals_[3].wait()
-    locals_[4].wait()
-    for step in (1, 2, 3):
-        att_wait(step)
-    advance(5, 9)
+    forward(14.5)
+    for copy in locals_[2:5]:
+        copy.wait()
+    forward(16)
+    wait_of(att_all.at[pl.ds(0, 3)], att_sem.at[1])
+    forward(18)
 
     tile = 256
 
@@ -515,7 +516,10 @@
         mixed[:, span] = value
         return squares + jnp.sum(value * value, axis=-1, keepdims=True)
 
-    squares = lax.fori_loop(0, wide // tile, project, jnp.zeros((own, 1), F32))
+    squares = lax.fori_loop(0, wide // tile // 2, project, jnp.zeros((own, 1), F32))
+    forward(19.5)
+    squares = lax.fori_loop(wide // tile // 2, wide // tile, project, squares)
+    forward(21)
     scale = lax.rsqrt(squares / wide + 1e-06)
     own_rows = pl.ds(aligned(me, own), own)
 
@@ -523,9 +527,8 @@
         place = normed.at[
             pl.ds(aligned(source, own), own), pl.ds(aligned(owner_at(order), depth), depth)
         ]
-        return remote(
-            place, place, norm_send.at[order, slot], norm_recv.at[order, source], {"tp": target}
-        )
+        link = 0 if slot == 0 else 1
+        return remote(place, place, norm_send.at[slot], norm_recv.at[order, link], {"tp": target})
 
     for order in range(n):
         span = pl.ds(aligned(owner_at(order), depth), depth)
@@ -534,17 +537,19 @@
         norm_copy(1, order, me, partner).start()
 
     locals_[5].wait()
-    plan = ((7, 11), (10, 13), (11, 16), (13, 19))
+    clocks = (29.2, 33.2, 37.4, 41.6)
     for order in range(n):
         owner = owner_at(order)
-        advance(*plan[order])
-        norm_copy(2, order, across, across).wait_recv()
+        forward(clocks[order] - 3)
+        forward(clocks[order] - 1.5)
+        span = pl.ds(aligned(owner, depth), depth)
+        wait_of(normed.at[own_rows, span], norm_recv.at[order, 0])
         norm_copy(2, order, across, partner).start()
-        if order != 1:
-            advance(*(count + 1 for count in plan[order]))
-        take(4 * order, 4 * min(order + order % 2, n - 1))
-        norm_copy(2, order, partner, partner).wait_recv()
-        norm_copy(2, order, diagonal, partner).wait_recv()
+        forward(clocks[order])
+        if order:
+            advance(order * CHUNKS, min(order + order % 2, n - 1) * CHUNKS)
+            wait_of(half_of(0, owner, 1 - y), y_up.at[slot_of(owner, z)])
+        wait_of(normed.at[pl.ds(0, 2 * own), span], norm_recv.at[order, 1])
 
         def up_step(index, carry, owner=owner, order=order):
             span = pl.ds(aligned(index, tile), tile)
@@ -580,7 +585,7 @@
         return remote(
             terms.at[which, pl.ds(aligned(group, own), own), pl.ds(0, size)],
             pair_in.at[which, slot, :, pl.ds(0, size)],
-            pair_send.at[which, slot],
+            send_sem.at[0],
             pair_recv.at[which, slot],
             {"tp": partner},
         )
@@ -590,22 +595,35 @@
         return remote(
             chip_sum.at[which, :, pl.ds(0, size)],
             peer_in.at[which, :, pl.ds(0, size)],
-            peer_send.at[which],
+            send_sem.at[1],
             peer_recv.at[which],
             {"tp": across},
         )
 
-    def multiply(which):
-        owner, block, offset, size = place_of(which)
-        if size == part:
-            weight = jnp.concatenate([down_buf[owner, block, half] for half in range(2)], axis=1)
-        else:
-            weight = down_buf[owner, block, y if which == last else 1 - y]
-        terms[which, :, 0:size] = jnp.dot(
-            hidden[...], weight, preferred_element_type=F32
-        ).astype(BF16)
+    half_depth = hidden.shape[1] // 2
+
+    def weight_of(which, start, size):
+        owner, block, _, lanes = place_of(which)
+        rows_ = pl.ds(start, size)
+        if lanes == part:
+            return jnp.concatenate([down_buf[owner, block, half, rows_] for half in range(2)], axis=1)
+        return down_buf[owner, block, y if which == last else 1 - y, rows_]
+
+    def half_wait(which, half):
+        owner, block = unit_at(min(which, last) - 2)
+        wait_of(
+            down_buf.at[owner, block, 1 - y, pl.ds(half * half_depth, half_depth)],
+            y_down.at[slot_of(owner, z), block * 2 + half],
+        )
+
+    def give(which, value):
+        terms[which, :, 0 : value.shape[1]] = value.astype(BF16)
         pair_copy(which, 1).start()
         pair_copy(which, 0).start()
+
+    def multiply(which):
+        weight = weight_of(which, 0, 2 * half_depth)
+        give(which, jnp.dot(hidden[...], weight, preferred_element_type=F32))
 
     def combine(which):
         size = place_of(which)[3]
@@ -616,9 +634,17 @@
         ).astype(BF16)
         peer_copy(which).start()
 
+    def target_of(which):
+        owner, block, offset, size = place_of(which)
+        return pl.ds(pl.multiple_of(owner * width + block * part + offset, size), size)
+
+    def out_copy(which):
+        target = target_of(which)
+        return pltpu.make_async_copy(out_buf.at[:, target], out.at[:, target], send_sem.at[2])
+
     def finish(which):
-        owner, block, offset, size = place_of(which)
-        target = pl.ds(pl.multiple_of(owner * width + block * part + offset, size), size)
+        size = place_of(which)[3]
+        target = target_of(which)
         peer_copy(which).wait_recv()
         pair_copy(which, 0).wait_recv()
         value = (
@@ -626,62 +652,77 @@
             + pair_in[which, 0, :, 0:size].astype(F32)
             + peer_in[which, :, 0:size].astype(F32)
         )
-        out[:, target] = (mixed[:, target] + value).astype(BF16)
-
-    first = 4 * (n - 1)
-    for which in range(blocks + 1):
-        ready = first + 2 * (min(which, last) - 1)
-        if which < 2:
-            advance(first + 3 + which, first + 7 + which)
-        elif which != last:
-            for step in range(2):
-                advance(ready - 1 + step + LEAD, ready + 6)
-                take(ready - 1 + step, ready - 1 + step)
-        else:
-            advance(ready, ready + 6)
+        out_buf[:, target] = (mixed[:, target] + value).astype(BF16)
+        out_copy(which).start()
+
+    forward(46)
+    multiply(0)
+    forward(47.5)
+    multiply(1)
+    combine(0)
+    forward(49)
+    combine(1)
+    forward(50)
+    for which in range(2, last):
+        ready = total + (which - 1) * PIECES
+        advance(ready + PIECES, ready + 3 * PIECES)
+        half_wait(which, 0)
+        half_wait(which, 1)
         multiply(which)
+        advance(ready + PIECES * 3 // 2, ready + 3 * PIECES)
         combine(which)
-        if which == 1:
-            advance(first + 5, first + 9)
-        if which:
-            finish(which - 1)
+        finish(which - 2)
+    multiply(last)
+    half_wait(last, 0)
+    acc[:, 0:lane] = jnp.dot(
+        hidden[:, 0:half_depth],
+        weight_of(blocks, 0, half_depth),
+        preferred_element_type=F32,
+    )
+    combine(last)
+    finish(last - 2)
+    finish(last - 1)
+    half_wait(last, 1)
+    rest = jnp.dot(
+        hidden[:, half_depth:],
+        weight_of(blocks, half_depth, half_depth),
+        preferred_element_type=F32,
+    )
+    give(blocks, acc[:, 0:lane] + rest)
+    combine(blocks)
+    finish(last)
     finish(blocks)
 
-    for step in (1, 2, 3):
-        att_copy(step).wait_send()
-    for order in range(n):
-        norm_copy(0, order, me, across).wait_send()
-        norm_copy(1, order, me, partner).wait_send()
-        norm_copy(2, order, across, partner).wait_send()
-    for which in range(blocks + 1):
-        pair_copy(which, 0).wait_send()
-        pair_copy(which, 1).wait_send()
-        peer_copy(which).wait_send()
+    wait_of(out_buf, send_sem.at[2])
+    wait_of(pair_in.at[pl.ds(0, blocks)], send_sem.at[0])
+    wait_of(chip_sum.at[pl.ds(0, blocks)], send_sem.at[1])
+    wait_of(att_all.at[pl.ds(0, 3)], att_sem.at[0])
+    for slot in range(3):
+        wait_of(normed.at[own_rows, :], norm_send.at[slot])
 
     @pl.when(z < n - 1)
     def _():
-        tail_copy(0).wait_send()
-        tail_copy(1).wait_send()
+        wait_of(kv_buf.at[:, :, pl.ds(0, WINDOW)], tail_sem.at[0])
 
     for weight in range(2):
 
         @pl.when(is_end)
         def _():
-            each_piece(lambda index: twin_copy(weight, index).wait_send())
+            wait_of(half_of(weight, z, 1 - y), twin_send.at[weight])
 
         for owner in range(n):
 
             @pl.when((z >= owner) & (z < n - 1))
             def _():
-                each_piece(lambda index: z_copy(weight, owner, index, 1).wait_send())
+                wait_of(half_of(weight, owner, y), z_send.at[weight, owner])
 
             @pl.when((z <= owner) & (z > 0))
             def _():
-                each_piece(lambda index: z_copy(weight, owner, index, 0).wait_send())
+                wait_of(half_of(weight, owner, y), z_send.at[weight, z_slot(owner, 0)])
 
             @pl.when((z != owner) & jnp.logical_not(has_twin(owner)))
             def _():
-                each_piece(lambda index: y_copy(weight, owner, index).wait_send())
+                wait_of(half_of(weight, owner, y), y_send.at[weight, slot_of(owner, z)])
 
 
 def fused_body(
@@ -711,18 +752,20 @@
             hbm,
             hbm,
             hbm,
-            pl.BlockSpec(memory_space=pltpu.SMEM),
             hbm,
             hbm,
-            pl.BlockSpec(memory_space=pltpu.VMEM),
+            hbm,
+            hbm,
             hbm,
             hbm,
         ],
-        out_specs=pl.BlockSpec(memory_space=pltpu.VMEM),
+        out_specs=hbm,
         scratch_shapes=[
+            pltpu.SMEM(sink_logits.shape, F32),
+            pltpu.VMEM((1, wide), F32),
+            vmem(own, wide),
             vmem(rows, head_cols),
-            vmem(HEAD_DIM, rows + WINDOW),
-            vmem(HEAD_DIM, rows + WINDOW),
+            vmem(2, HEAD_DIM, rows + WINDOW),
             vmem(head_cols, rows + WINDOW),
             vmem(head_cols, rows + WINDOW),
             vmem(rows, head_cols),
@@ -739,20 +782,19 @@
             vmem(2 * n + 1, 2, own, part),
             vmem(2 * n + 1, own, part),
             vmem(2 * n + 1, own, part),
-            dma(10),
+            dma(8),
             dma(2),
+            dma(2, n + 1),
             dma(2),
-            dma(2, 2, n, CHUNKS),
-            dma(2, CHUNKS),
-            dma(2, n, CHUNKS),
-            dma(2, n, 2, CHUNKS),
+            dma(2, n - 1),
+            dma(2, n - 1, CHUNKS),
+            dma(n - 1),
+            dma(n - 1, 4),
+            dma(2),
             dma(3),
-            dma(4),
-            dma(n, 3),
-            dma(n, 4),
+            dma(n, 2),
+            dma(3),
             dma(2 * n + 1, 2),
-            dma(2 * n + 1, 2),
-            dma(2 * n + 1),
             dma(2 * n + 1),
         ],
         compiler_params=pltpu.CompilerParams(

time: 90.3 us -> 85.9 us (0.951)
  Pallas kernels: 89.2 us -> 84.9 us
    pallas_call x1, Pallas kernels: 89.2 us -> 84.9 us  [fused_body(): pl.pallas_call(functools.partial(layer_kernel, n), out_shape=pltpu.VMEM((...]
where the time goes in v2:
time: 85.9 us; the launch traced here: 85.8 us
  Pallas kernels  84.9 us (99%)
  local copies, waits for them, and re-layouts  0.88 us (1%)
    pallas_call x1, Pallas kernels, fused_body(): pl.pallas_call(functools.partial(layer_kernel, n), out_shape=pltpu.VMEM((...  84.9 us

profile of v2, /device:TPU:0, one launch (start us, length us, event | category | flops | bytes accessed | tf_op | source)
XLA Modules:
  0.0 85.8 jit_solution(6773403742754368587)
XLA Ops:
  0.0 84.9 %shard_map.91 = bf16[192,2048]{1,0:T(8,128)(2,1)S(1)} custom-call(bf16[768,256]{1,0:T(8,128)(2,1)} %queries.1, bf16[64,768]{1,0:T(8,128)(2,1)} %bitcast.3, bf16[64,768]{1,0:T(8,128)(2,1)} %bitcast.4, f32[4]{0:T(128)} %sink_in.1, bf16[1024,2048]{1,0:T(8,128)(2,1)} %out_weight.1, bf16[192,2048]{1,0:T(8,128)(2,1)} %residual.1, f32[1,2048]{1,0:T(1,128)} %bitcast.5, ...), custom_call_target="tpu_custom_call" | custom-call | tf_op jit(solution)/shard_map/pallas_call | solution.py:748
  84.9 0.9 %copy.11 = bf16[192,2048]{1,0:T(8,128)(2,1)} copy(bf16[192,2048]{1,0:T(8,128)(2,1)S(1)} %shard_map.91) | data formatting | bytes 1572864

commit v3 on v2

--- a/solution.py
+++ b/solution.py
@@ -320,13 +320,17 @@
             {"sp": z + 1},
         )
 
+    @pl.when((z > 0) & (far_sign > 0))
+    def _():
+        send_own(0, 0)
+
     @pl.when(z < n - 1)
     def _():
         tail_copy(0).start()
         tail_copy(1).start()
         send_own(0, 1)
 
-    @pl.when(z > 0)
+    @pl.when((z > 0) & (far_sign < 0))
     def _():
         send_own(0, 0)
 
@@ -364,7 +368,11 @@
         def _():
             z_copy(weight, owner, index, 0).start()
 
-        @pl.when(jnp.logical_not(has_twin(owner)))
+        skip = has_twin(owner)
+        if weight == 1:
+            skip |= is_end & (owner == n - 1 - z) & (index // (PIECES // 2) == 3)
+
+        @pl.when(jnp.logical_not(skip))
         def _():
             y_copy(weight, owner, index).start()
 
@@ -566,7 +574,9 @@
                 acc[:, span] = value
             return carry
 
-        lax.fori_loop(0, cols // tile, up_step, 0)
+        lax.fori_loop(0, cols // tile // 2, up_step, 0)
+        forward(clocks[order] + 0.6)
+        lax.fori_loop(cols // tile // 2, cols // tile, up_step, 0)
 
     blocks = 2 * n
     last = blocks - 1
@@ -609,6 +619,17 @@
             return jnp.concatenate([down_buf[owner, block, half, rows_] for half in range(2)], axis=1)
         return down_buf[owner, block, y if which == last else 1 - y, rows_]
 
+    def relay():
+        owner, block = unit_at(last - 2)
+        place = down_buf.at[owner, block, 1 - y, pl.ds(half_depth, half_depth)]
+        return remote(
+            place,
+            place,
+            twin_send.at[2],
+            y_down.at[slot_of(owner, z - far_sign), block * 2 + 1],
+            {"sp": z - far_sign},
+        )
+
     def half_wait(which, half):
         owner, block = unit_at(min(which, last) - 2)
         wait_of(
@@ -663,33 +684,49 @@
     forward(49)
     combine(1)
     forward(50)
+    def partial(which, half):
+        start = half * half_depth
+        return jnp.dot(
+            hidden[:, start : start + half_depth],
+            weight_of(which, start, half_depth),
+            preferred_element_type=F32,
+        )
+
     for which in range(2, last):
         ready = total + (which - 1) * PIECES
-        advance(ready + PIECES, ready + 3 * PIECES)
+        final = which == last - 1
+        advance(ready + PIECES // (2 if final else 1), ready + 3 * PIECES)
         half_wait(which, 0)
         half_wait(which, 1)
         multiply(which)
+        if final:
+
+            @pl.when(jnp.logical_not(is_end))
+            def _():
+                half_wait(last, 1)
+                relay().start()
+
+            break
         advance(ready + PIECES * 3 // 2, ready + 3 * PIECES)
         combine(which)
         finish(which - 2)
-    multiply(last)
+    acc[:, 0:lane] = partial(last, 0)
+    combine(last - 1)
+    advance(2 * total, 2 * total)
+    give(last, acc[:, 0:lane] + partial(last, 1))
+
+    @pl.when(is_end)
+    def _():
+        half_wait(last, 1)
+
+    acc[:, 0:lane] = partial(blocks, 1)
+    finish(last - 3)
+    combine(last)
     half_wait(last, 0)
-    acc[:, 0:lane] = jnp.dot(
-        hidden[:, 0:half_depth],
-        weight_of(blocks, 0, half_depth),
-        preferred_element_type=F32,
-    )
-    combine(last)
+    give(blocks, acc[:, 0:lane] + partial(blocks, 0))
     finish(last - 2)
+    combine(blocks)
     finish(last - 1)
-    half_wait(last, 1)
-    rest = jnp.dot(
-        hidden[:, half_depth:],
-        weight_of(blocks, half_depth, half_depth),
-        preferred_element_type=F32,
-    )
-    give(blocks, acc[:, 0:lane] + rest)
-    combine(blocks)
     finish(last)
     finish(blocks)
 
@@ -710,6 +747,12 @@
         def _():
             wait_of(half_of(weight, z, 1 - y), twin_send.at[weight])
 
+        if weight == 1:
+
+            @pl.when(jnp.logical_not(is_end))
+            def _():
+                relay().wait_send()
+
         for owner in range(n):
 
             @pl.when((z >= owner) & (z < n - 1))
@@ -720,9 +763,18 @@
             def _():
                 wait_of(half_of(weight, owner, y), z_send.at[weight, z_slot(owner, 0)])
 
-            @pl.when((z != owner) & jnp.logical_not(has_twin(owner)))
+            short = is_end & (owner == n - 1 - z) & (weight == 1)
+
+            @pl.when((z != owner) & jnp.logical_not(has_twin(owner) | short))
             def _():
                 wait_of(half_of(weight, owner, y), y_send.at[weight, slot_of(owner, z)])
+
+            if weight == 1:
+
+                @pl.when(short)
+                def _():
+                    part_of = up_buf.at[pl.ds(0, 3 * depth // 8), :]
+                    wait_of(part_of, y_send.at[weight, slot_of(owner, z)])
 
 
 def fused_body(
@@ -785,7 +837,7 @@
             dma(8),
             dma(2),
             dma(2, n + 1),
-            dma(2),
+            dma(3),
             dma(2, n - 1),
             dma(2, n - 1, CHUNKS),
             dma(n - 1),

time: 85.9 us -> 84.2 us (0.980)
  Pallas kernels: 84.9 us -> 83.1 us
    pallas_call x1, Pallas kernels: 84.9 us -> 83.1 us  [fused_body(): pl.pallas_call(functools.partial(layer_kernel, n), out_shape=pltpu.VMEM((...]
where the time goes in v3:
time: 84.2 us; the launch traced here: 84 us
  Pallas kernels  83.1 us (99%)
  local copies, waits for them, and re-layouts  0.88 us (1%)
    pallas_call x1, Pallas kernels, fused_body(): pl.pallas_call(functools.partial(layer_kernel, n), out_shape=pltpu.VMEM((...  83.1 us

profile of v3, /device:TPU:0, one launch (start us, length us, event | category | flops | bytes accessed | tf_op | source)
XLA Modules:
  0.0 84.0 jit_solution(17386199511498498242)
XLA Ops:
  0.0 83.1 %shard_map.91 = bf16[192,2048]{1,0:T(8,128)(2,1)S(1)} custom-call(bf16[768,256]{1,0:T(8,128)(2,1)} %queries.1, bf16[64,768]{1,0:T(8,128)(2,1)} %bitcast.3, bf16[64,768]{1,0:T(8,128)(2,1)} %bitcast.4, f32[4]{0:T(128)} %sink_in.1, bf16[1024,2048]{1,0:T(8,128)(2,1)} %out_weight.1, bf16[192,2048]{1,0:T(8,128)(2,1)} %residual.1, f32[1,2048]{1,0:T(1,128)} %bitcast.5, ...), custom_call_target="tpu_custom_call" | custom-call | tf_op jit(solution)/shard_map/pallas_call | solution.py:800
  83.1 0.9 %copy.11 = bf16[192,2048]{1,0:T(8,128)(2,1)} copy(bf16[192,2048]{1,0:T(8,128)(2,1)S(1)} %shard_map.91) | data formatting | bytes 1572864

commit v4 on v3

--- a/solution.py
+++ b/solution.py
@@ -102,7 +102,7 @@
 
 
 PIECES = 4
-HOP = 4.7
+HOP = 4.3
 PACE = 2.8
 CHUNKS = 2 * PIECES
 F32 = jnp.float32
@@ -695,10 +695,15 @@
     for which in range(2, last):
         ready = total + (which - 1) * PIECES
         final = which == last - 1
-        advance(ready + PIECES // (2 if final else 1), ready + 3 * PIECES)
+        advance(ready + PIECES * 3 // 4, ready + 3 * PIECES)
         half_wait(which, 0)
+        if final:
+            acc[:, lane : lane + part] = partial(which, 0)
         half_wait(which, 1)
-        multiply(which)
+        if final:
+            give(which, acc[:, lane : lane + part] + partial(which, 1))
+        else:
+            multiply(which)
         if final:
 
             @pl.when(jnp.logical_not(is_end))
@@ -720,10 +725,10 @@
         half_wait(last, 1)
 
     acc[:, 0:lane] = partial(blocks, 1)
-    finish(last - 3)
-    combine(last)
     half_wait(last, 0)
     give(blocks, acc[:, 0:lane] + partial(blocks, 0))
+    combine(last)
+    finish(last - 3)
     finish(last - 2)
     combine(blocks)
     finish(last - 1)

time: 84.2 us -> 83.6 us (level)
  no operation moved by 1% of the time
where the time goes in v4:
time: 83.6 us; the launch traced here: 83.5 us
  Pallas kernels  82.6 us (99%)
  local copies, waits for them, and re-layouts  0.88 us (1%)
    pallas_call x1, Pallas kernels, fused_body(): pl.pallas_call(functools.partial(layer_kernel, n), out_shape=pltpu.VMEM((...  82.6 us

profile of v4, /device:TPU:0, one launch (start us, length us, event | category | flops | bytes accessed | tf_op | source)
XLA Modules:
  0.0 83.5 jit_solution(6739525101565659400)
XLA Ops:
  0.0 82.6 %shard_map.91 = bf16[192,2048]{1,0:T(8,128)(2,1)S(1)} custom-call(bf16[768,256]{1,0:T(8,128)(2,1)} %queries.1, bf16[64,768]{1,0:T(8,128)(2,1)} %bitcast.3, bf16[64,768]{1,0:T(8,128)(2,1)} %bitcast.4, f32[4]{0:T(128)} %sink_in.1, bf16[1024,2048]{1,0:T(8,128)(2,1)} %out_weight.1, bf16[192,2048]{1,0:T(8,128)(2,1)} %residual.1, f32[1,2048]{1,0:T(1,128)} %bitcast.5, ...), custom_call_target="tpu_custom_call" | custom-call | tf_op jit(solution)/shard_map/pallas_call | solution.py:805
  82.6 0.9 %copy.11 = bf16[192,2048]{1,0:T(8,128)(2,1)} copy(bf16[192,2048]{1,0:T(8,128)(2,1)S(1)} %shard_map.91) | data formatting | bytes 1572864

commit v5 on v4

--- a/solution.py
+++ b/solution.py
@@ -524,10 +524,12 @@
         mixed[:, span] = value
         return squares + jnp.sum(value * value, axis=-1, keepdims=True)
 
-    squares = lax.fori_loop(0, wide // tile // 2, project, jnp.zeros((own, 1), F32))
-    forward(19.5)
-    squares = lax.fori_loop(wide // tile // 2, wide // tile, project, squares)
-    forward(21)
+    squares = jnp.zeros((own, 1), F32)
+    for step in range(4):
+        squares = lax.fori_loop(
+            step * wide // tile // 4, (step + 1) * wide // tile // 4, project, squares
+        )
+        forward(18.7 + 0.75 * step)
     scale = lax.rsqrt(squares / wide + 1e-06)
     own_rows = pl.ds(aligned(me, own), own)
 
@@ -596,7 +598,7 @@
             terms.at[which, pl.ds(aligned(group, own), own), pl.ds(0, size)],
             pair_in.at[which, slot, :, pl.ds(0, size)],
             send_sem.at[0],
-            pair_recv.at[which, slot],
+            pair_recv.at[which],
             {"tp": partner},
         )
 
@@ -648,7 +650,7 @@
 
     def combine(which):
         size = place_of(which)[3]
-        pair_copy(which, 1).wait_recv()
+        wait_of(pair_in.at[which, :, :, pl.ds(0, size)], pair_recv.at[which])
         other = pl.ds(aligned(across, own), own)
         chip_sum[which, :, 0:size] = (
             terms[which, other, 0:size].astype(F32) + pair_in[which, 1, :, 0:size].astype(F32)
@@ -667,7 +669,6 @@
         size = place_of(which)[3]
         target = target_of(which)
         peer_copy(which).wait_recv()
-        pair_copy(which, 0).wait_recv()
         value = (
             terms[which, own_rows, 0:size].astype(F32)
             + pair_in[which, 0, :, 0:size].astype(F32)
@@ -851,7 +852,7 @@
             dma(3),
             dma(n, 2),
             dma(3),
-            dma(2 * n + 1, 2),
+            dma(2 * n + 1),
             dma(2 * n + 1),
         ],
         compiler_params=pltpu.CompilerParams(

time: 83.6 us -> 83.6 us (level)
  no operation moved by 1% of the time
where the time goes in v5:
time: 83.6 us; the launch traced here: 83.4 us
  Pallas kernels  82.5 us (99%)
  local copies, waits for them, and re-layouts  0.88 us (1%)
    pallas_call x1, Pallas kernels, fused_body(): pl.pallas_call(functools.partial(layer_kernel, n), out_shape=pltpu.VMEM((...  82.5 us

profile of v5, /device:TPU:0, one launch (start us, length us, event | category | flops | bytes accessed | tf_op | source)
XLA Modules:
  0.0 83.4 jit_solution(16027528861798084839)
XLA Ops:
  0.0 82.5 %shard_map.91 = bf16[192,2048]{1,0:T(8,128)(2,1)S(1)} custom-call(bf16[768,256]{1,0:T(8,128)(2,1)} %queries.1, bf16[64,768]{1,0:T(8,128)(2,1)} %bitcast.3, bf16[64,768]{1,0:T(8,128)(2,1)} %bitcast.4, f32[4]{0:T(128)} %sink_in.1, bf16[1024,2048]{1,0:T(8,128)(2,1)} %out_weight.1, bf16[192,2048]{1,0:T(8,128)(2,1)} %residual.1, f32[1,2048]{1,0:T(1,128)} %bitcast.5, ...), custom_call_target="tpu_custom_call" | custom-call | tf_op jit(solution)/shard_map/pallas_call | solution.py:806
  82.6 0.9 %copy.11 = bf16[192,2048]{1,0:T(8,128)(2,1)} copy(bf16[192,2048]{1,0:T(8,128)(2,1)S(1)} %shard_map.91) | data formatting | bytes 1572864
